TPU v7x, 512 devices: a whole 4x4x16 slice. The times are simulated.
512 devices in a mesh: fs: 16 (over y, x), tp: 32 (over z, core).
Axes of the slice: x: 4, y: 4, z: 16, core: 2. Of those that a mesh axis runs over, the one named last changes fastest.
Arguments:
- normed: bfloat16 [2048, 49152], P('tp', 'fs'), may hold values from -6 to 6
- key_cot: bfloat16 [2048, 49152], P('tp', 'fs'), may hold values from -6 to 6
- first_map: bfloat16 [2048, 49152], P('tp', 'fs'), may hold values from -6 to 6
- second_map: bfloat16 [2048, 49152], P('tp', 'fs'), may hold values from -6 to 6
- lambdas: float32 [8], replicated, may hold values from 0.3 to 0.8
- factor: bfloat16 [2048, 256], replicated, may hold values from -0.125 to 0.125
- key_master: float32 [2048, 2048], P('fs', 'tp'), may hold values from -0.125 to 0.125
- value_master: float32 [2048, 2048], P('fs', 'tp'), may hold values from -0.125 to 0.125
- key_first: float32 [256, 2048], P('fs', 'tp'), may hold values from -6 to 6
- key_second: float32 [256, 2048], P('fs', 'tp'), may hold values from 0.5 to 2
- value_first: float32 [256, 2048], P('fs', 'tp'), may hold values from -6 to 6
- value_second: float32 [256, 2048], P('fs', 'tp'), may hold values from 0.5 to 2
Outputs:
- key_master_new: float32 [2048, 2048], P('fs', 'tp')
- value_master_new: float32 [2048, 2048], P('fs', 'tp')
- key_copy: bfloat16 [2048, 2048], P(None, 'tp')
- value_copy: bfloat16 [2048, 2048], P(None, 'tp')
- key_first_new: float32 [256, 2048], P('fs', 'tp')
- key_second_new: float32 [256, 2048], P('fs', 'tp')
- value_first_new: float32 [256, 2048], P('fs', 'tp')
- value_second_new: float32 [256, 2048], P('fs', 'tp')
All inputs are finite; a program needn't handle non-finite values.
Results may differ from a plain program's by a relative error of at most 0.0012.
Values may be sent and summed in bfloat16 or wider, within the bound.
No kernel may reach another device: no remote copies, remote signals or barrier semaphores. Data moves between devices by JAX's collectives and lax.ppermute only.
A program may use at most 64 MiB of HBM per device.

v0:
```python
import math
import jax
import jax.numpy as jnp
from jax import lax
from jax.sharding import Mesh
from jax.sharding import PartitionSpec as P

VALUE_DIM = 256
TP = ("tp_0", "tp_1")
FS = ("fs_0", "fs_1")
FS_TP = ("fs_0", "fs_1", "tp_0", "tp_1")


def cut_along(shard, dim, size):
    lengths = shard.shape
    pieces = shard.reshape(*lengths[:dim], size, lengths[dim] // size, *lengths[dim + 1 :])
    return jnp.moveaxis(pieces, dim, 0)


def summed_on_arrival(shard, axis, dim):
    size = lax.axis_size(axis)
    pieces = lax.all_to_all(cut_along(shard, dim, size), axis, 0, 0, tiled=True)
    return jnp.sum(pieces, axis=0)


def sent_to_all(shard, axis):
    size = lax.axis_size(axis)
    return lax.all_to_all(
        jnp.broadcast_to(shard[None], (size, *shard.shape)), axis, 0, 0, tiled=True
    )


def in_order(pieces, dim):
    lengths = list(pieces.shape[1:])
    lengths[dim] *= pieces.shape[0]
    return jnp.moveaxis(pieces, 0, dim).reshape(lengths)


def collect(shard, axis, dim):
    pieces = sent_to_all(shard, axis)
    return in_order(pieces, dim)


def over_axes(shard, axes):
    for axis in axes:
        shard = lax.psum(shard, axis)
    return shard


def local(
    normed,
    key_cot,
    first_map,
    second_map,
    lambdas,
    factor,
    key_master,
    value_master,
    key_first,
    key_second,
    value_first,
    value_second,
):
    width = first_map.shape[0]
    key_width = key_cot.shape[0]
    heads = lambdas.shape[0]
    tok_local = normed.shape[1]
    rows_here = lax.axis_index(TP) * width + lax.iota(jnp.int32, width)
    owners = rows_here // VALUE_DIM
    picked = (owners[:, None] == lax.iota(jnp.int32, heads)[None, :]).astype(jnp.float32)
    row_lambda = jnp.sum(picked * lambdas[None, :], axis=1)
    value_cot = (
        first_map.astype(jnp.float32) - row_lambda[:, None] * second_map.astype(jnp.float32)
    ).astype(jnp.bfloat16)
    cotangents = jnp.concatenate([key_cot, value_cot], axis=0)
    norm_scale = 1.0 / math.sqrt(tok_local * lax.axis_size(FS))
    fs_rows = key_master.shape[0]
    factor_rows = lax.dynamic_slice_in_dim(factor, lax.axis_index(FS) * fs_rows, fs_rows, 0).astype(
        jnp.float32
    )
    term = lax.dot_general(
        lax.all_gather(normed, TP, axis=0, tiled=True),
        cotangents,
        (((1,), (1,)), ((), ())),
        preferred_element_type=jnp.float32,
    )
    gradient = summed_on_arrival(term, FS, 0) * norm_scale
    partial_value = lax.dot_general(
        factor_rows, gradient, (((0,), (0,)), ((), ())), precision=lax.Precision.HIGHEST
    )
    small = summed_on_arrival(partial_value, FS, 0)
    first = jnp.concatenate([key_first, value_first], axis=1)
    second = jnp.concatenate([key_second, value_second], axis=1)
    first_new = 0.8 * first + 0.2 * small
    second_new = 0.9 * second + 0.1 * small * small
    direction = first_new / (jnp.sqrt(second_new) + 1e-06)
    directions = collect(direction, FS, 0)
    raw = jnp.dot(factor_rows, directions, precision=lax.Precision.HIGHEST)
    key_raw = raw[:, :key_width]
    value_raw = raw[:, key_width:]
    squares = (
        over_axes(jnp.sum(key_raw * key_raw), FS_TP),
        over_axes(jnp.sum(value_raw * value_raw), FS_TP),
    )
    key_cells = fs_rows * lax.axis_size(FS) * key_width * lax.axis_size(TP)
    value_cells = fs_rows * lax.axis_size(FS) * width * lax.axis_size(TP)
    key_update = key_raw / jnp.sqrt(squares[0] / key_cells + 0.01)
    value_update = value_raw / jnp.sqrt(squares[1] / value_cells + 0.01)
    key_new = 0.998 * key_master - 0.02 * key_update
    value_new = 0.998 * value_master - 0.02 * value_update
    halves = jnp.concatenate([key_new, value_new], axis=1).astype(jnp.bfloat16)
    copies = collect(halves, FS, 0)
    return (
        key_new,
        value_new,
        copies[:, :key_width],
        copies[:, key_width:],
        first_new[:, :key_width],
        second_new[:, :key_width],
        first_new[:, key_width:],
        second_new[:, key_width:],
    )


def solution(mesh):
    split = Mesh(mesh.devices.reshape(4, 4, 16, 2), ("fs_0", "fs_1", "tp_0", "tp_1"))
    placed = (
        P(TP, FS),
        P(TP, FS),
        P(TP, FS),
        P(TP, FS),
        P(),
        P(),
        P(FS, TP),
        P(FS, TP),
        P(FS, TP),
        P(FS, TP),
        P(FS, TP),
        P(FS, TP),
    )
    return jax.shard_map(
        local,
        mesh=split,
        in_specs=placed,
        out_specs=(
            P(FS, TP),
            P(FS, TP),
            P(None, TP),
            P(None, TP),
            P(FS, TP),
            P(FS, TP),
            P(FS, TP),
            P(FS, TP),
        ),
        check_vma=False,
    )
```

profile of v0, /device:TPU:1, one launch (start us, length us, event | category | flops | bytes accessed | tf_op | source)
XLA Modules:
  0.0 239.1 jit_solution(16993545285375096101)
XLA Ops:
  7.3 0.7 all-gather.2.cloned.1.call-update
  8.0 0.7 select_reduce_fusion
  8.7 1.3 subtract_convert_fusion
  10.0 92.9 %all-gather.2.cloned.1.call-done = bf16[2048,3072]{1,0:T(8,128)(2,1)} async-done(((bf16[64,3072]{1,0:T(8,128)(2,1)}), bf16[2048,3072]{1,0:T(8,128)(2,1)}) %all-gather.2.cloned.1.call-update) | async-done | bytes 12582928 | tf_op jit(solution)/shard_map/all_gather | solution.py:82
  103.0 9.0 %convolution_bitcast_fusion = f32[16,16,8,128]{3,2,1,0:T(8,128)S(1)} fusion(bf16[2048,3072]{1,0:T(8,128)(2,1)} %all-gather.2.cloned.1.call-done, bf16[64,3072]{1,0:T(8,128)(2,1)S(1)} %subtract_convert_fusion, bf16[64,3072]{1,0:T(8,128)(2,1)} %param.13), kind=kOutput, calls=%fused_computation | convolution fusion | flops 1612185600 | bytes 14417920 | tf_op jit(solution)/shard_map/dot_general | solution.py:81
  112.0 1.1 copy.35
  113.1 6.5 %all-to-all-start = ((f32[16,128,128]{1,2,0:T(8,128)}), f32[16,128,128]{1,2,0:T(8,128)S(1)}, u32[]{:S(2)}, u32[]{:S(2)}) async-start(f32[16,128,128]{1,2,0:T(8,128)} %bitcast.10), calls=%async_computation | async-start | bytes 2097152 | tf_op jit(solution)/shard_map/all_to_all | solution.py:22
  119.6 16.4 %all-to-all-done = f32[16,128,128]{1,2,0:T(8,128)S(1)} async-done(((f32[16,128,128]{1,2,0:T(8,128)}), f32[16,128,128]{1,2,0:T(8,128)S(1)}, u32[]{:S(2)}, u32[]{:S(2)}) %all-to-all-start) | async-done | bytes 1048608 | tf_op jit(solution)/shard_map/all_to_all | solution.py:22
  136.4 11.1 %all_to_all.20 = f32[16,16,128]{2,1,0:T(8,128)S(1)} all-to-all(f32[16,16,128]{2,1,0:T(8,128)S(1)} %bitcast.13), channel_id=1, replica_groups=mesh['fs_0'=4,'fs_1'=4,'tp_0'=16,'tp_1'=2] {'fs_0','fs_1'}, dimensions={0} | all-to-all | bytes 262144 | tf_op jit(solution)/shard_map/all_to_all | solution.py:22
  147.7 9.9 %all_to_all.21 = f32[16,16,128]{2,1,0:T(8,128)S(1)} all-to-all(f32[16,16,128]{2,1,0:T(8,128)S(1)} %broadcast_in_dim.4), channel_id=1, replica_groups=mesh['fs_0'=4,'fs_1'=4,'tp_0'=16,'tp_1'=2] {'fs_0','fs_1'}, dimensions={0} | all-to-all | bytes 262144 | tf_op jit(solution)/shard_map/all_to_all | solution.py:28
  157.6 0.3 fusion.5
  157.9 0.6 multiply_reduce_fusion
  158.5 7.3 %all-reduce.2 = (f32[]{:T(128)}, f32[]{:T(128)}) all-reduce(f32[]{:T(128)} %get-tuple-element.25, f32[]{:T(128)} %get-tuple-element.24), channel_id=1, replica_groups=mesh['fs_0'=4,'fs_1'=4,'tp_0'=16,'tp_1'=2] {'fs_0'}, use_global_device_ids=true, to_apply=%region_4.5 | all-reduce | flops 2 | bytes 16 | tf_op jit(solution)/shard_map/psum | solution.py:46
  165.8 7.5 %all-reduce.1 = (f32[]{:T(128)}, f32[]{:T(128)}) all-reduce(f32[]{:T(128)} %get-tuple-element.30, f32[]{:T(128)} %get-tuple-element.31), channel_id=1, replica_groups=mesh['fs_0'=4,'fs_1'=4,'tp_0'=16,'tp_1'=2] {'fs_1'}, use_global_device_ids=true, to_apply=%region_5.6 | all-reduce | flops 2 | bytes 16 | tf_op jit(solution)/shard_map/psum | solution.py:46
  173.3 22.4 %all-reduce = (f32[]{:T(128)}, f32[]{:T(128)}) all-reduce(f32[]{:T(128)} %get-tuple-element.28, f32[]{:T(128)} %get-tuple-element.29), channel_id=1, replica_groups=mesh['fs_0'=4,'fs_1'=4,'tp_0'=16,'tp_1'=2] {'tp_0'}, use_global_device_ids=true, to_apply=%region_6.7 | all-reduce | flops 2 | bytes 16 | tf_op jit(solution)/shard_map/psum | solution.py:46
  195.6 16.8 %all-reduce.3 = (f32[]{:T(128)}, f32[]{:T(128)}) all-reduce(f32[]{:T(128)} %get-tuple-element.26, f32[]{:T(128)} %get-tuple-element.27), channel_id=1, replica_groups=mesh['fs_0'=4,'fs_1'=4,'tp_0'=16,'tp_1'=2] {'tp_1'}, use_global_device_ids=true, to_apply=%region_7.8 | all-reduce | flops 2 | bytes 16 | tf_op jit(solution)/shard_map/psum | solution.py:46
  213.8 0.6 fusion.16
  214.5 0.9 broadcast_in_dim.5
  215.4 3.6 %all-to-all-start.3 = ((bf16[16,128,128]{1,2,0:T(8,128)(2,1)}), bf16[16,128,128]{1,2,0:T(8,128)(2,1)S(1)}, u32[]{:S(2)}, u32[]{:S(2)}) async-start(bf16[16,128,128]{1,2,0:T(8,128)(2,1)} %broadcast_in_dim.5), calls=%async_computation.3 | async-start | bytes 1048576 | tf_op jit(solution)/shard_map/all_to_all | solution.py:28
  219.0 0.7 fusion.20
  219.6 10.3 %all-to-all-done.3 = bf16[16,128,128]{1,2,0:T(8,128)(2,1)S(1)} async-done(((bf16[16,128,128]{1,2,0:T(8,128)(2,1)}), bf16[16,128,128]{1,2,0:T(8,128)(2,1)S(1)}, u32[]{:S(2)}, u32[]{:S(2)}) %all-to-all-start.3) | async-done | bytes 524320 | tf_op jit(solution)/shard_map/all_to_all | solution.py:28
  229.9 0.3 copy.29
  230.4 0.9 copy.31
  231.3 0.9 copy.30
  (23 shorter events, 0.8 us)
Async XLA Ops:
  7.2 129.0 %copy-start = (bf16[2048,256]{1,0:T(8,128)(2,1)S(1)}, bf16[2048,256]{1,0:T(8,128)(2,1)}, u32[]{:S(2)}) copy-start(bf16[2048,256]{1,0:T(8,128)(2,1)} %param.17) | copy-start | bytes 3145732
  7.2 140.4 %copy-start.3 = (f32[16,64]{1,0:T(8,128)S(1)}, f32[16,64]{1,0:T(8,128)}, u32[]{:S(2)}) copy-start(f32[16,64]{1,0:T(8,128)} %param.23) | copy-start | bytes 12292
  7.2 140.4 %copy-start.5 = (f32[16,64]{1,0:T(8,128)S(1)}, f32[16,64]{1,0:T(8,128)}, u32[]{:S(2)}) copy-start(f32[16,64]{1,0:T(8,128)} %param.22) | copy-start | bytes 12292
  7.2 140.4 %copy-start.4 = (f32[16,64]{1,0:T(8,128)S(1)}, f32[16,64]{1,0:T(8,128)}, u32[]{:S(2)}) copy-start(f32[16,64]{1,0:T(8,128)} %param.21) | copy-start | bytes 12292
  7.2 140.4 %copy-start.6 = (f32[16,64]{1,0:T(8,128)S(1)}, f32[16,64]{1,0:T(8,128)}, u32[]{:S(2)}) copy-start(f32[16,64]{1,0:T(8,128)} %param.20) | copy-start | bytes 12292
  7.2 206.6 %copy-start.1 = (f32[128,64]{0,1:T(8,128)S(1)}, f32[128,64]{0,1:T(8,128)}, u32[]{:S(2)}) copy-start(f32[128,64]{0,1:T(8,128)} %param.19) | copy-start | bytes 98308
  7.2 206.6 %copy-start.2 = (f32[128,64]{0,1:T(8,128)S(1)}, f32[128,64]{0,1:T(8,128)}, u32[]{:S(2)}) copy-start(f32[128,64]{0,1:T(8,128)} %param.18) | copy-start | bytes 98308
  7.2 95.7 %all-gather.2.cloned.1.call-start = ((), (), s32[]{:S(2)}) async-start(), calls=%async_computation.4 | async-start | bytes 12976128 | tf_op jit(solution)/shard_map/all_gather | solution.py:82
  113.1 23.0 %all-to-all-start = ((f32[16,128,128]{1,2,0:T(8,128)}), f32[16,128,128]{1,2,0:T(8,128)S(1)}, u32[]{:S(2)}, u32[]{:S(2)}) async-start(f32[16,128,128]{1,2,0:T(8,128)} %bitcast.10), calls=%async_computation | async-start | bytes 2097152 | tf_op jit(solution)/shard_map/all_to_all | solution.py:22
  215.4 14.5 %all-to-all-start.3 = ((bf16[16,128,128]{1,2,0:T(8,128)(2,1)}), bf16[16,128,128]{1,2,0:T(8,128)(2,1)S(1)}, u32[]{:S(2)}, u32[]{:S(2)}) async-start(bf16[16,128,128]{1,2,0:T(8,128)(2,1)} %broadcast_in_dim.5), calls=%async_computation.3 | async-start | bytes 1048576 | tf_op jit(solution)/shard_map/all_to_all | solution.py:28
Sparse Core Ops, SparseCore 0:
  10.2 92.7 all-gather.1
where the time goes:
time: 240 us; the launch traced here: 239 us
  waiting for transfers between devices  120 us (50%)
  blocking collectives  74.9 us (31%)
  between operations  15.6 us (6%)
  starting transfers between devices  10.1 us (4%)
  matrix products  9.54 us (4%)
  local copies, waits for them, and re-layouts  5 us (2%)
  other arithmetic  3.48 us (1%)
    all_gather x1, waiting for transfers between devices, local(): lax.all_gather(normed, TP, axis=0, tiled=True)  92.9 us
    psum x4, blocking collectives, over_axes(): shard = lax.psum(shard, axis)  53.9 us
    all_to_all x1, waiting for transfers between devices, summed_on_arrival(): pieces = lax.all_to_all(cut_along(shard, dim, size), axis, 0, 0, tiled=True)  16.4 us
    all_to_all x1, blocking collectives, summed_on_arrival(): pieces = lax.all_to_all(cut_along(shard, dim, size), axis, 0, 0, tiled=True)  11.1 us
    all_to_all x1, waiting for transfers between devices, sent_to_all(): lax.all_to_all(jnp.broadcast_to(shard[None], (size, *shard.shape)), axis,...  10.3 us
    all_to_all x1, blocking collectives, sent_to_all(): lax.all_to_all(jnp.broadcast_to(shard[None], (size, *shard.shape)), axis,...  9.93 us
    dot_general x1, matrix products, local(): lax.dot_general(lax.all_gather(normed, TP, axis=0, tiled=True), cotangent...  8.99 us
    all_to_all x1, starting transfers between devices, summed_on_arrival(): pieces = lax.all_to_all(cut_along(shard, dim, size), axis, 0, 0, tiled=True)  6.53 us
  transfers between devices with their start and end apart: 3, of which 3 were waited for; matrix products, arithmetic and copies ran while one was open for 1% of the time, Pallas kernels for 0%

commit v1 on v0

--- a/solution.py
+++ b/solution.py
@@ -43,7 +43,7 @@
 
 def over_axes(shard, axes):
     for axis in axes:
-        shard = lax.psum(shard, axis)
+        shard = jnp.sum(lax.all_gather(shard, axis), axis=0)
     return shard
 
 

time: 240 us -> 257 us (1.071)
  local copies, waits for them, and re-layouts: 5 us -> 21.9 us
  blocking collectives: 74.9 us -> 62.4 us
  waiting for transfers between devices: 120 us -> 125 us
  other arithmetic: 3.48 us -> 8.29 us
  starting transfers between devices: 10.1 us -> 13.6 us
    psum x4 -> x0, blocking collectives: 53.9 us -> none  [over_axes(): shard = lax.psum(shard, axis)]
    unnamed x0 -> x4, blocking collectives: none -> 51.3 us
    unnamed x16 -> x36, local copies, waits for them, and re-layouts: 1.84 us -> 18.1 us
    all_to_all x1 -> x0, blocking collectives: 9.93 us -> none  [sent_to_all(): lax.all_to_all(jnp.broadcast_to(shard[None], (size, *shard.shape)), axis,...]
    reduce_sum x0 -> x8, other arithmetic: none -> 4.81 us  [over_axes(): shard = jnp.sum(lax.all_gather(shard, axis), axis=0)]
    all_to_all x1 -> x2, waiting for transfers between devices: 10.3 us -> 14.5 us  [sent_to_all(): lax.all_to_all(jnp.broadcast_to(shard[None], (size, *shard.shape)), axis,...]
    all_to_all x1 -> x2, starting transfers between devices: 3.57 us -> 7.08 us  [sent_to_all(): lax.all_to_all(jnp.broadcast_to(shard[None], (size, *shard.shape)), axis,...]
  transfers between devices with their start and end apart: 3 -> 4, of which waited for: 3 -> 4; matrix products, arithmetic and copies ran while one was open for 1% -> 2% of each run, Pallas kernels for 0% -> 0%
where the time goes in v1:
time: 257 us; the launch traced here: 256 us
  waiting for transfers between devices  125 us (49%)
  blocking collectives  62.4 us (24%)
  local copies, waits for them, and re-layouts  21.9 us (9%)
  between operations  15.6 us (6%)
  starting transfers between devices  13.6 us (5%)
  matrix products  9.54 us (4%)
  other arithmetic  8.29 us (3%)
    all_gather x1, waiting for transfers between devices, local(): lax.all_gather(normed, TP, axis=0, tiled=True)  92.9 us
    unnamed x4, blocking collectives  51.3 us
    unnamed x36, local copies, waits for them, and re-layouts  18.1 us
    all_to_all x1, waiting for transfers between devices, summed_on_arrival(): pieces = lax.all_to_all(cut_along(shard, dim, size), axis, 0, 0, tiled=True)  16.4 us
    all_to_all x2, waiting for transfers between devices, sent_to_all(): lax.all_to_all(jnp.broadcast_to(shard[None], (size, *shard.shape)), axis,...  14.5 us
    all_to_all x1, blocking collectives, summed_on_arrival(): pieces = lax.all_to_all(cut_along(shard, dim, size), axis, 0, 0, tiled=True)  11.1 us
    dot_general x1, matrix products, local(): lax.dot_general(lax.all_gather(normed, TP, axis=0, tiled=True), cotangent...  8.99 us
    all_to_all x2, starting transfers between devices, sent_to_all(): lax.all_to_all(jnp.broadcast_to(shard[None], (size, *shard.shape)), axis,...  7.08 us
  transfers between devices with their start and end apart: 4, of which 4 were waited for; matrix products, arithmetic and copies ran while one was open for 2% of the time, Pallas kernels for 0%

profile of v1, /device:TPU:1, one launch (start us, length us, event | category | flops | bytes accessed | tf_op | source)
XLA Modules:
  0.0 256.1 jit_solution(11242671892659536923)
XLA Ops:
  8.7 1.3 subtract_convert_fusion
  10.0 92.9 %all-gather.2.cloned.1.call-done = bf16[2048,3072]{1,0:T(8,128)(2,1)} async-done(((bf16[64,3072]{1,0:T(8,128)(2,1)}), bf16[2048,3072]{1,0:T(8,128)(2,1)}) %all-gather.2.cloned.1.call-update) | async-done | bytes 12582928 | tf_op jit(solution)/shard_map/all_gather | solution.py:82
  103.0 9.0 %convolution_bitcast_fusion = f32[16,16,8,128]{3,2,1,0:T(8,128)S(1)} fusion(bf16[2048,3072]{1,0:T(8,128)(2,1)} %all-gather.2.cloned.1.call-done, bf16[64,3072]{1,0:T(8,128)(2,1)S(1)} %subtract_convert_fusion, bf16[64,3072]{1,0:T(8,128)(2,1)} %param.13), kind=kOutput, calls=%fused_computation | convolution fusion | flops 1612185600 | bytes 14417920 | tf_op jit(solution)/shard_map/dot_general | solution.py:81
  113.1 6.5 %all-to-all-start = ((f32[16,128,128]{1,2,0:T(8,128)}), f32[16,128,128]{1,2,0:T(8,128)S(1)}, u32[]{:S(2)}, u32[]{:S(2)}) async-start(f32[16,128,128]{1,2,0:T(8,128)} %bitcast.22), calls=%async_computation | async-start | bytes 2097152 | tf_op jit(solution)/shard_map/all_to_all | solution.py:22
  119.6 16.4 %all-to-all-done = f32[16,128,128]{1,2,0:T(8,128)S(1)} async-done(((f32[16,128,128]{1,2,0:T(8,128)}), f32[16,128,128]{1,2,0:T(8,128)S(1)}, u32[]{:S(2)}, u32[]{:S(2)}) %all-to-all-start) | async-done | bytes 1048608 | tf_op jit(solution)/shard_map/all_to_all | solution.py:22
  136.4 11.1 %all_to_all.20 = f32[16,16,128]{2,1,0:T(8,128)S(1)} all-to-all(f32[16,16,128]{2,1,0:T(8,128)S(1)} %bitcast.25), channel_id=1, replica_groups=mesh['fs_0'=4,'fs_1'=4,'tp_0'=16,'tp_1'=2] {'fs_0','fs_1'}, dimensions={0} | all-to-all | bytes 262144 | tf_op jit(solution)/shard_map/all_to_all | solution.py:22
  148.4 3.5 %all-to-all-start.2 = ((f32[16,16,128]{2,1,0:T(8,128)}), f32[16,16,128]{2,1,0:T(8,128)S(1)}, u32[]{:S(2)}, u32[]{:S(2)}) async-start(f32[16,16,128]{2,1,0:T(8,128)} %broadcast_in_dim.4), calls=%async_computation.2 | async-start | bytes 262144 | tf_op jit(solution)/shard_map/all_to_all | solution.py:28
  151.9 1.3 dynamic-slice
  154.4 4.3 %all-to-all-done.2 = f32[16,16,128]{2,1,0:T(8,128)S(1)} async-done(((f32[16,16,128]{2,1,0:T(8,128)}), f32[16,16,128]{2,1,0:T(8,128)S(1)}, u32[]{:S(2)}, u32[]{:S(2)}) %all-to-all-start.2) | async-done | bytes 131104 | tf_op jit(solution)/shard_map/all_to_all | solution.py:28
  159.6 1.4 dynamic-update-slice.4
  161.0 1.4 dynamic-update-slice
  162.4 1.3 dynamic-slice.2
  163.7 6.5 %all-reduce.10 = (f32[4]{0:T(128)S(1)}, f32[4]{0:T(128)S(1)}) all-reduce(f32[4]{0:T(128)S(1)} %dynamic-update-slice, f32[4]{0:T(128)S(1)} %dynamic-update-slice.4), channel_id=1, replica_groups=mesh['fs_0'=4,'fs_1'=4,'tp_0'=16,'tp_1'=2] {'fs_0'}, use_global_device_ids=true, to_apply=%add | all-reduce | flops 8 | bytes 64
  171.4 1.4 dynamic-update-slice.5
  172.8 1.4 dynamic-update-slice.1
  175.5 6.9 %all-reduce.9 = (f32[4]{0:T(128)S(1)}, f32[4]{0:T(128)S(1)}) all-reduce(f32[4]{0:T(128)S(1)} %dynamic-update-slice.1, f32[4]{0:T(128)S(1)} %dynamic-update-slice.5), channel_id=1, replica_groups=mesh['fs_0'=4,'fs_1'=4,'tp_0'=16,'tp_1'=2] {'fs_1'}, use_global_device_ids=true, to_apply=%add.1 | all-reduce | flops 8 | bytes 64
  183.6 1.4 dynamic-update-slice.6
  185.0 1.4 dynamic-update-slice.2
  186.4 21.7 %all-reduce.8 = (f32[16]{0:T(128)S(1)}, f32[16]{0:T(128)S(1)}) all-reduce(f32[16]{0:T(128)S(1)} %dynamic-update-slice.2, f32[16]{0:T(128)S(1)} %dynamic-update-slice.6), channel_id=1, replica_groups=mesh['fs_0'=4,'fs_1'=4,'tp_0'=16,'tp_1'=2] {'tp_0'}, use_global_device_ids=true, to_apply=%add.2 | all-reduce | flops 32 | bytes 256
  209.3 1.4 dynamic-update-slice.7
  210.7 1.4 dynamic-update-slice.3
  212.1 16.2 %all-reduce.11 = (f32[2]{0:T(128)S(1)}, f32[2]{0:T(128)S(1)}) all-reduce(f32[2]{0:T(128)S(1)} %dynamic-update-slice.3, f32[2]{0:T(128)S(1)} %dynamic-update-slice.7), channel_id=1, replica_groups=mesh['fs_0'=4,'fs_1'=4,'tp_0'=16,'tp_1'=2] {'tp_1'}, use_global_device_ids=true, to_apply=%add.3 | all-reduce | flops 4 | bytes 32
  232.4 3.6 %all-to-all-start.3 = ((bf16[16,128,128]{1,2,0:T(8,128)(2,1)}), bf16[16,128,128]{1,2,0:T(8,128)(2,1)S(1)}, u32[]{:S(2)}, u32[]{:S(2)}) async-start(bf16[16,128,128]{1,2,0:T(8,128)(2,1)} %broadcast_in_dim.5), calls=%async_computation.3 | async-start | bytes 1048576 | tf_op jit(solution)/shard_map/all_to_all | solution.py:28
  236.7 10.3 %all-to-all-done.3 = bf16[16,128,128]{1,2,0:T(8,128)(2,1)S(1)} async-done(((bf16[16,128,128]{1,2,0:T(8,128)(2,1)}), bf16[16,128,128]{1,2,0:T(8,128)(2,1)S(1)}, u32[]{:S(2)}, u32[]{:S(2)}) %all-to-all-start.3) | async-done | bytes 524320 | tf_op jit(solution)/shard_map/all_to_all | solution.py:28
  (52 shorter events, 16.5 us)
Async XLA Ops:
  7.2 129.0 %copy-start = (bf16[2048,256]{1,0:T(8,128)(2,1)S(1)}, bf16[2048,256]{1,0:T(8,128)(2,1)}, u32[]{:S(2)}) copy-start(bf16[2048,256]{1,0:T(8,128)(2,1)} %param.17) | copy-start | bytes 3145732
  7.2 140.4 %copy-start.6 = (f32[16,64]{1,0:T(8,128)S(1)}, f32[16,64]{1,0:T(8,128)}, u32[]{:S(2)}) copy-start(f32[16,64]{1,0:T(8,128)} %param.20) | copy-start | bytes 12292
  7.2 140.4 %copy-start.4 = (f32[16,64]{1,0:T(8,128)S(1)}, f32[16,64]{1,0:T(8,128)}, u32[]{:S(2)}) copy-start(f32[16,64]{1,0:T(8,128)} %param.21) | copy-start | bytes 12292
  7.2 140.4 %copy-start.5 = (f32[16,64]{1,0:T(8,128)S(1)}, f32[16,64]{1,0:T(8,128)}, u32[]{:S(2)}) copy-start(f32[16,64]{1,0:T(8,128)} %param.22) | copy-start | bytes 12292
  7.2 140.4 %copy-start.3 = (f32[16,64]{1,0:T(8,128)S(1)}, f32[16,64]{1,0:T(8,128)}, u32[]{:S(2)}) copy-start(f32[16,64]{1,0:T(8,128)} %param.23) | copy-start | bytes 12292
  7.2 223.6 %copy-start.2 = (f32[128,64]{0,1:T(8,128)S(1)}, f32[128,64]{0,1:T(8,128)}, u32[]{:S(2)}) copy-start(f32[128,64]{0,1:T(8,128)} %param.18) | copy-start | bytes 98308
  7.2 223.6 %copy-start.1 = (f32[128,64]{0,1:T(8,128)S(1)}, f32[128,64]{0,1:T(8,128)}, u32[]{:S(2)}) copy-start(f32[128,64]{0,1:T(8,128)} %param.19) | copy-start | bytes 98308
  7.2 95.7 %all-gather.2.cloned.1.call-start = ((), (), s32[]{:S(2)}) async-start(), calls=%async_computation.4 | async-start | bytes 12976128 | tf_op jit(solution)/shard_map/all_gather | solution.py:82
  113.1 23.0 %all-to-all-start = ((f32[16,128,128]{1,2,0:T(8,128)}), f32[16,128,128]{1,2,0:T(8,128)S(1)}, u32[]{:S(2)}, u32[]{:S(2)}) async-start(f32[16,128,128]{1,2,0:T(8,128)} %bitcast.22), calls=%async_computation | async-start | bytes 2097152 | tf_op jit(solution)/shard_map/all_to_all | solution.py:22
  148.4 10.3 %all-to-all-start.2 = ((f32[16,16,128]{2,1,0:T(8,128)}), f32[16,16,128]{2,1,0:T(8,128)S(1)}, u32[]{:S(2)}, u32[]{:S(2)}) async-start(f32[16,16,128]{2,1,0:T(8,128)} %broadcast_in_dim.4), calls=%async_computation.2 | async-start | bytes 262144 | tf_op jit(solution)/shard_map/all_to_all | solution.py:28
  232.4 14.5 %all-to-all-start.3 = ((bf16[16,128,128]{1,2,0:T(8,128)(2,1)}), bf16[16,128,128]{1,2,0:T(8,128)(2,1)S(1)}, u32[]{:S(2)}, u32[]{:S(2)}) async-start(bf16[16,128,128]{1,2,0:T(8,128)(2,1)} %broadcast_in_dim.5), calls=%async_computation.3 | async-start | bytes 1048576 | tf_op jit(solution)/shard_map/all_to_all | solution.py:28
Sparse Core Ops, SparseCore 0:
  10.2 92.7 all-gather.1
